TPU v7x, 128 devices: a whole 4x4x4 slice. The times are simulated.
128 devices in a mesh: sp: 16 (over z, y), tp: 8 (over x, core).
Axes of the slice: x: 4, y: 4, z: 4, core: 2. Of those that a mesh axis runs over, the one named last changes fastest.
Arguments:
- query_proj: bfloat16 [16384, 2048], P('sp', 'tp'), may hold values from -6 to 6
- key_proj: bfloat16 [16384, 2048], P('sp', 'tp'), may hold values from -6 to 6
- value_proj: bfloat16 [16384, 4096], P('sp', 'tp'), may hold values from -6 to 6
- gate_proj: bfloat16 [16384, 4096], P('sp', 'tp'), may hold values from -6 to 6
- log_decay: float32 [16384, 8], P('sp', 'tp'), may hold values from -0.75 to 0, as said below
- residual: bfloat16 [16384, 2048], P('sp'), may hold values from -4 to 4
- out_weight: bfloat16 [4096, 2048], P('tp'), may hold values from -0.09375 to 0.09375
- norm_gain: float32 [2, 2048], replicated, may hold values from 0.1 to 1.9
- norm_bias: float32 [2, 2048], replicated, may hold values from -1.5 to 1.5
- up_gate: bfloat16 [2048, 5632], P('sp', 'tp'), may hold values from -0.125 to 0.125
- up_value: bfloat16 [2048, 5632], P('sp', 'tp'), may hold values from -0.125 to 0.125
- conv_weight: float32 [2, 3, 5632], P(None, None, 'tp'), may hold values from -3 to 3
- conv_bias: float32 [2, 5632], P(None, 'tp'), may hold values from -1.5 to 1.5
- down_weight: bfloat16 [5632, 2048], P('tp', 'sp'), may hold values from -0.078125 to 0.078125
Outputs:
- layer_output: bfloat16 [16384, 2048], P(('sp', 'tp'))
Inputs may be any that keep to these rules, and one draw needn't show every extreme that they name: `log_decay`: all entries are negative.
All inputs are finite; a program needn't handle non-finite values.
Results may differ from a plain program's by a relative error of at most 0.023.
Values may be sent and summed in bfloat16 or wider, within the bound.
No kernel may reach another device: no remote copies, remote signals or barrier semaphores. Data moves between devices by JAX's collectives and lax.ppermute only.
A program may use at most 128 MiB of HBM per device.

v0:
```python
import jax
import jax.numpy as jnp
from jax import lax
from jax.sharding import Mesh
from jax.sharding import PartitionSpec as P

BLOCK = 256
SP = ("sp_0", "sp_1")
SP_TP = ("sp_0", "sp_1", "tp")
alpha_scale = 8.0**0.25
rope_base = 10000.0
tiny_stabilizer = 1e-05


def turned_gather(arrays, axis, dims):
    turned = [jnp.moveaxis(a, dim, 0) for a, dim in zip(arrays, dims)]
    both = jnp.concatenate([t.reshape(len(t), -1) for t in turned], axis=1)
    out, at, finished = (lax.all_gather(both, axis, axis=0, tiled=True), 0, [])
    for t, dim in zip(turned, dims):
        piece = out[:, at : at + t[0].size].reshape(-1, *t.shape[1:])
        finished.append(jnp.moveaxis(piece, 0, dim))
        at += t[0].size
    return tuple(finished)


def neutral_like(x, identity):
    return jax.tree.map(
        lambda a, e: jnp.broadcast_to(jnp.asarray(e, a.dtype), a.shape), x, identity
    )


def entering(x, axes, combine, identity):
    before = start = neutral_like(x, identity)
    subtotal = x
    for axis in reversed(axes):
        length, position = (lax.axis_size(axis), lax.axis_index(axis))
        pieces = jax.tree.map(
            lambda part, kind: lax.all_gather(part.astype(kind), axis),
            subtotal,
            (jnp.bfloat16, jnp.bfloat16),
        )
        inside, subtotal = (start, start)
        for k in range(length):
            passed = k < position
            subtotal = combine(
                subtotal, jax.tree.map(lambda part, own: part[k].astype(own.dtype), pieces, x)
            )
            inside = jax.tree.map(lambda new, old: jnp.where(passed, new, old), subtotal, inside)
        before = combine(inside, before)
    return before


def passed_along(x, axis, by):
    length = lax.axis_size(axis)
    pairs = [(i, i + by) for i in range(length) if 0 <= i + by < length]
    return lax.ppermute(x, axis, pairs)


def rotate(vectors, positions):
    head_width = vectors.shape[-1]
    half_width = head_width // 2
    inverse_freq = rope_base ** (-2.0 * jnp.arange(half_width, dtype=jnp.float32) / head_width)
    angles = positions[:, None] * inverse_freq[None, :]
    cosine = jnp.cos(angles)[:, None, :]
    sine_part = jnp.sin(angles)[:, None, :]
    front = vectors[..., :half_width]
    second = vectors[..., half_width:]
    return jnp.concatenate(
        [front * cosine - second * sine_part, front * sine_part + second * cosine], axis=-1
    )


def layer_norm(values, gain, shift):
    average = values.mean(-1, keepdims=True)
    spread = jnp.square(values - average).mean(-1, keepdims=True)
    return (values - average) * lax.rsqrt(spread + tiny_stabilizer) * gain + shift


def block_parts(query_tile, lookup_piece, payload_piece, log_blk):
    cum_log = jnp.cumsum(log_blk, axis=0)
    cum_heads = cum_log.T
    log_gap = cum_heads[:, :, None] - cum_heads[:, None, :]
    offsets = jnp.arange(log_blk.shape[0])
    causal = (offsets[:, None] >= offsets[None, :])[None]
    weight = jnp.where(causal, jnp.exp(jnp.where(causal, log_gap, 0.0)), 0.0)
    score_matrix = jnp.einsum(
        "jka,ska->kjs", query_tile, lookup_piece, preferred_element_type=jnp.float32
    )
    segment_scaling = (score_matrix * weight).astype(jnp.bfloat16)
    within = jnp.einsum(
        "htm,mhe->the", segment_scaling, payload_piece, preferred_element_type=jnp.float32
    )
    block_total = cum_log[-1]
    to_end = jnp.exp(block_total[None, :] - cum_log)
    faded_lookup_vector = (lookup_piece.astype(jnp.float32) * to_end[:, :, None]).astype(
        jnp.bfloat16
    )
    summand_term = jnp.einsum(
        "ajo,ajd->jod", faded_lookup_vector, payload_piece, preferred_element_type=jnp.float32
    )
    scaled_query = (query_tile.astype(jnp.float32) * jnp.exp(cum_log)[:, :, None]).astype(
        jnp.bfloat16
    )
    return (within, scaled_query, summand_term, jnp.exp(block_total))


def causal_conv(rows, edge_rows, taps, shift):
    padded = jnp.concatenate([edge_rows, rows], axis=0).astype(jnp.float32)
    length = rows.shape[0]
    result = shift[None, :] + padded[0:length] * taps[0]
    result = result + padded[1 : length + 1] * taps[1]
    return result + padded[2 : length + 2] * taps[2]


def combine(earlier, later):
    return (earlier[0] * later[0], later[0][:, None, None] * earlier[1] + later[1])


def shards(
    query_proj,
    key_proj,
    value_proj,
    gate_proj,
    log_decay,
    residual,
    out_weight,
    norm_gain,
    norm_bias,
    up_gate,
    up_value,
    conv_weight,
    conv_bias,
    down_weight,
):
    tok_rows = query_proj.shape[0]
    head_count = log_decay.shape[1]
    key_width = query_proj.shape[1] // head_count
    value_width = value_proj.shape[1] // head_count
    full_gate, full_value, full_down = turned_gather(
        (up_gate, up_value, down_weight), SP, (0, 0, 1)
    )
    positions = (lax.axis_index(SP) * tok_rows + jnp.arange(tok_rows)).astype(jnp.float32)
    query_rot = rotate(
        query_proj.astype(jnp.float32).reshape(tok_rows, head_count, key_width), positions
    ).astype(jnp.bfloat16)
    key_rot = (
        rotate(key_proj.astype(jnp.float32).reshape(tok_rows, head_count, key_width), positions)
        * key_width ** (-0.5)
    ).astype(jnp.bfloat16)
    block_count = tok_rows // BLOCK
    asking_segments = query_rot.reshape(block_count, BLOCK, head_count, key_width)
    key_blocks = key_rot.reshape(block_count, BLOCK, head_count, key_width)
    value_blocks = value_proj.reshape(block_count, BLOCK, head_count, value_width)
    log_blocks = log_decay.reshape(block_count, BLOCK, head_count)
    within, scaled_query, summand_term, block_decay = jax.vmap(block_parts)(
        asking_segments, key_blocks, value_blocks, log_blocks
    )

    def absorb(carry_state, pieces):
        return (pieces[1][:, None, None] * carry_state + pieces[0], None)

    zero_state = jnp.zeros((head_count, key_width, value_width), jnp.float32)
    own_state, _ = lax.scan(absorb, zero_state, (summand_term, block_decay))
    own_decay = jnp.prod(block_decay, axis=0)
    _, incoming = entering(
        (own_decay, own_state), SP, combine, (jnp.ones_like(own_decay), zero_state)
    )

    def advance(carry_state, pieces):
        carried = jnp.einsum(
            "thd,hde->the",
            pieces[0],
            carry_state.astype(jnp.bfloat16),
            preferred_element_type=jnp.float32,
        )
        return (pieces[2][:, None, None] * carry_state + pieces[1], carried)

    _, carried = lax.scan(advance, incoming, (scaled_query, summand_term, block_decay))
    mixed_heads = (within + carried).reshape(tok_rows, head_count, value_width)
    average = mixed_heads.mean(-1, keepdims=True)
    spread = jnp.square(mixed_heads - average).mean(-1, keepdims=True)
    standardized_rows = (mixed_heads - average) * lax.rsqrt(spread + tiny_stabilizer)
    gate_heads = gate_proj.astype(jnp.float32).reshape(tok_rows, head_count, value_width)
    gated_rows = (
        (jax.nn.silu(gate_heads) * standardized_rows)
        .astype(jnp.bfloat16)
        .reshape(tok_rows, head_count * value_width)
    )
    own_count = tok_rows // lax.axis_size("tp")
    partial_rows = jnp.dot(gated_rows, out_weight, preferred_element_type=jnp.float32)
    attended = lax.psum_scatter(
        partial_rows.astype(jnp.bfloat16), "tp", scatter_dimension=0, tiled=True
    ).astype(jnp.float32)
    own_residual = lax.dynamic_slice_in_dim(
        residual, lax.axis_index("tp") * own_count, own_count, 0
    )
    normed_own = layer_norm(
        alpha_scale * own_residual.astype(jnp.float32) + attended, norm_gain[0], norm_bias[0]
    ).astype(jnp.bfloat16)
    whole_rows = lax.all_gather(normed_own, "tp", axis=0, tiled=True)
    gate_up = jnp.dot(whole_rows, full_gate, preferred_element_type=jnp.float32)
    value_up = jnp.dot(whole_rows, full_value, preferred_element_type=jnp.float32)
    gate_up = gate_up.astype(jnp.bfloat16)
    value_up = value_up.astype(jnp.bfloat16)
    edges = jnp.concatenate([gate_up[tok_rows - 2 :], value_up[tok_rows - 2 :]], axis=0)
    edges = passed_along(edges, SP, 1)
    gate_edge, value_edge = (edges[:2], edges[2:])
    gate_conv = causal_conv(gate_up, gate_edge, conv_weight[0], conv_bias[0])
    value_conv = causal_conv(value_up, value_edge, conv_weight[1], conv_bias[1])
    activated = (jax.nn.gelu(gate_conv) * value_conv).astype(jnp.bfloat16)
    partial_ffn = jnp.dot(activated, full_down, preferred_element_type=jnp.float32)
    ffn_out = lax.psum_scatter(
        partial_ffn.astype(jnp.bfloat16), "tp", scatter_dimension=0, tiled=True
    ).astype(jnp.float32)
    return layer_norm(
        alpha_scale * normed_own.astype(jnp.float32) + ffn_out, norm_gain[1], norm_bias[1]
    ).astype(jnp.bfloat16)


def solution(mesh):
    torus = Mesh(mesh.devices.reshape(4, 4, mesh.shape["tp"]), ("sp_0", "sp_1", "tp"))
    return jax.shard_map(
        shards,
        mesh=torus,
        in_specs=(
            P(SP, "tp"),
            P(SP, "tp"),
            P(SP, "tp"),
            P(SP, "tp"),
            P(SP, "tp"),
            P(SP, None),
            P("tp", None),
            P(),
            P(),
            P(SP, "tp"),
            P(SP, "tp"),
            P(None, None, "tp"),
            P(None, "tp"),
            P("tp", SP),
        ),
        out_specs=P(SP_TP, None),
        check_vma=False,
    )
```

profile of v0, /device:TPU:0, one launch (start us, length us, event | category | flops | bytes accessed | tf_op | source)
XLA Modules:
  0.0 314.5 jit_solution(11302256274251141249)
XLA Ops:
  7.4 2.4 reduce-window.6
  11.8 3.1 fusion.56
  17.7 9.8 %while.24 = (s32[]{:T(128)}, f32[1,256,512]{2,1,0:T(8,128)S(1)}, f32[4,1]{0,1:T(1,128)S(1)}, f32[4,1,256,512]{3,2,1,0:T(8,128)}, s32[]{:T(128)}, /*index=5*/s32[]{:T(128)}) while((s32[]{:T(128)}, f32[1,256,512]{2,1,0:T(8,128)S(1)}, f32[4,1]{0,1:T(1,128)S(1)}, f32[4,1,256,512]{3,2,1,0:T(8,128)}, s32[]{:T(128)}, ...), condition=%wide.region_4.5_spmd.clone, body=%wide.region_3.4_spmd.clone.sunk | while | flops 393219 | bytes 1572971 | solution.py:163
  31.0 10.8 %all-reduce = bf16[4]{0:T(256)(128)(2,1)S(1)} all-reduce(bf16[4]{0:T(256)(128)(2,1)S(1)} %dynamic-update-slice), channel_id=1, replica_groups=mesh['sp_0'=4,'sp_1'=4,'tp'=8] {'sp_1'}, use_global_device_ids=true, to_apply=%add | all-reduce | flops 4 | bytes 16
  43.2 11.9 %all-gather.13.cloned.1.call-done = bf16[4,256,512]{2,1,0:T(8,128)(2,1)} async-done(((bf16[1,256,512]{2,1,0:T(8,128)(2,1)}), bf16[4,256,512]{2,1,0:T(8,128)(2,1)}) %all-gather.13.cloned.1.call-update) | async-done | bytes 1048592 | tf_op jit(solution)/shard_map/all_gather | solution.py:38
  55.0 4.0 %fusion.70 = bf16[1,1,256,512]{3,2,1,0:T(8,128)(2,1)} fusion(f32[]{:T(128)} %bitcast.39, f32[]{:T(128)} %bitcast.40, f32[]{:T(128)} %bitcast.41, f32[]{:T(128)} %bitcast.42, bf16[4,256,512]{2,1,0:T(8,128)(2,1)} %all-gather.13.cloned.1.call-done), kind=kLoop, calls=%fused_computation.102 | loop fusion | flops 1572864 | bytes 1310736 | tf_op jit(solution)/shard_map/convert_element_type | solution.py:38
  61.8 10.7 %all-reduce.1 = bf16[4]{0:T(256)(128)(2,1)S(1)} all-reduce(bf16[4]{0:T(256)(128)(2,1)S(1)} %dynamic-update-slice.1), channel_id=2, replica_groups=mesh['sp_0'=4,'sp_1'=4,'tp'=8] {'sp_0'}, use_global_device_ids=true, to_apply=%add.1 | all-reduce | flops 4 | bytes 16
  80.2 3.6 %all-gather.7.cloned.1.call-done = bf16[4,1,256,512]{3,2,1,0:T(8,128)(2,1)} async-done(((bf16[1,1,256,512]{3,2,1,0:T(8,128)(2,1)}), bf16[4,1,256,512]{3,2,1,0:T(8,128)(2,1)}) %all-gather.7.cloned.1.call-update) | async-done | bytes 1048592 | tf_op jit(solution)/shard_map/all_gather | solution.py:38
  83.8 3.9 %fusion.69 = f32[1,256,512]{2,1,0:T(8,128)S(1)} fusion(bf16[4,1,256,512]{3,2,1,0:T(8,128)(2,1)} %all-gather.7.cloned.1.call-done, f32[]{:T(128)} %bitcast.39, f32[]{:T(128)} %bitcast.40, f32[]{:T(128)} %bitcast.41, f32[]{:T(128)} %bitcast.42, f32[]{:T(128)} %bitcast.33, f32[]{:T(128)S(6)} %convert.26, f32[]{:T(128)S(6)} %convert.27, f32[]{:T(128)} %bitcast.38, ...), kind=kLoop, calls=%fused_computation.99 | loop fusion | flops 4194304 | bytes 2621484 | tf_op jit(solution)/shard_map/add | solution.py:116
  87.7 17.8 %while.23 = (s32[]{:T(128)}, f32[1,256,512]{2,1,0:T(8,128)S(1)}, f32[4,256,1,512]{3,1,2,0:T(8,128)}, f32[4,1]{0,1:T(1,128)S(1)}, f32[4,1,256,512]{3,2,1,0:T(8,128)}, /*index=5*/bf16[4,256,1,256]{3,1,2,0:T(8,128)(2,1)}, s32[]{:T(128)}) while((s32[]{:T(128)}, f32[1,256,512]{2,1,0:T(8,128)S(1)}, f32[4,256,1,512]{3,1,2,0:T(8,128)}, ...), condition=%wide.region_6.7_spmd, body=%wide.region_5.6_spmd.sunk | while | flops 67502080 | bytes 2753641 | solution.py:178
  105.5 4.2 %fusion.102 = (f32[4,256]{1,0:T(4,128)S(1)}, f32[4,256,1,512]{3,1,0,2:T(8,128)}) fusion(f32[4,256,1,512]{3,1,2,0:T(8,128)} %get-tuple-element.60, bf16[4,256,512]{2,1,0:T(8,128)(2,1)} %bitcast.150, bf16[4,256,128]{2,1,0:T(8,128)(2,1)} %bitcast.155, bf16[4,256,128]{2,1,0:T(8,128)(2,1)S(1)} %bitcast.153, f32[4,256]{1,0:T(4,128)S(1)} %get-tuple-element.145, ...), kind=kOutput, calls=%fused_computation.160 | convolution fusion | flops 406846464 | bytes 6889472 | tf_op jit(solution)/shard_map/vmap(htm,mhe->the)/dot_general | solution.py:90
  112.0 2.2 fusion.31
  114.2 4.3 %convolution_convert_fusion.1 = bf16[1024,2048]{1,0:T(8,128)(2,1)} fusion(bf16[1024,512]{1,0:T(8,128)(2,1)S(1)} %fusion.31, bf16[512,2048]{1,0:T(8,128)(2,1)S(1)} %copy-done), kind=kOutput, calls=%fused_computation.14 | convolution fusion | flops 2149580800 | bytes 7340032 | tf_op jit(solution)/shard_map/dot_general | solution.py:190
  120.6 36.8 %reduce-scatter.3.cloned.1.call-done = bf16[128,2048]{1,0:T(8,128)(2,1)} async-done(((bf16[1024,2048]{1,0:T(8,128)(2,1)}), bf16[128,2048]{1,0:T(8,128)(2,1)}) %reduce-scatter.3.cloned.1.call-update) | async-done | bytes 524304 | tf_op jit(solution)/shard_map/reduce_scatter | solution.py:191
  160.4 2.4 add_convert_fusion.1
  163.1 36.6 %all-gather.11.cloned.1.call-done = bf16[2048,2112]{0,1:T(8,128)(2,1)} async-done(((bf16[128,2112]{0,1:T(8,128)(2,1)}), bf16[2048,2112]{0,1:T(8,128)(2,1)}) %all-gather.11.cloned.1.call-update) | async-done | bytes 8650768 | tf_op jit(solution)/shard_map/all_gather | solution.py:18
  199.7 32.7 %all-gather.9.cloned.1.call-done = bf16[1024,2048]{1,0:T(8,128)(2,1)} async-done(((bf16[128,2048]{1,0:T(8,128)(2,1)}), bf16[1024,2048]{1,0:T(8,128)(2,1)}) %all-gather.9.cloned.1.call-update) | async-done | bytes 4194320 | tf_op jit(solution)/shard_map/all_gather | solution.py:200
  232.4 6.4 %fusion.32 = bf16[1024,704]{0,1:T(8,128)(2,1)S(1)} fusion(bf16[1024,2048]{1,0:T(8,128)(2,1)} %all-gather.9.cloned.1.call-done, bf16[2048,2112]{0,1:T(8,128)(2,1)} %all-gather.11.cloned.1.call-done), kind=kOutput, calls=%fused_computation.52 | convolution fusion | flops 2953510912 | bytes 8519680 | tf_op jit(solution)/shard_map/dot_general | solution.py:201
  239.0 5.0 %fusion.35 = bf16[1024,704]{0,1:T(8,128)(2,1)S(1)} fusion(bf16[1024,2048]{1,0:T(8,128)(2,1)S(1)} %copy-done.12, bf16[2048,2112]{0,1:T(8,128)(2,1)} %all-gather.11.cloned.1.call-done), kind=kOutput, calls=%fused_computation.53 | convolution fusion | flops 2953510912 | bytes 8519680 | tf_op jit(solution)/shard_map/dot_general | solution.py:202
  244.3 3.6 %collective-permute-start = (bf16[4,704]{0,1:T(8,128)(2,1)S(1)}, bf16[4,704]{0,1:T(8,128)(2,1)S(1)}, u32[]{:S(2)}, u32[]{:S(2)}) collective-permute-start(bf16[4,704]{0,1:T(8,128)(2,1)S(1)} %pad_maximum_fusion.1), channel_id=1, source_target_pairs={{0,8},{8,16},{16,24},{24,32},{32,40},{40,48},{48,56},{56,64},{64,7... | collective-permute-start | bytes 16904 | tf_op jit(solution)/shard_map/ppermute | solution.py:56
  247.9 3.9 %collective-permute-done = bf16[4,704]{0,1:T(8,128)(2,1)S(1)} collective-permute-done((bf16[4,704]{0,1:T(8,128)(2,1)S(1)}, bf16[4,704]{0,1:T(8,128)(2,1)S(1)}, u32[]{:S(2)}, u32[]{:S(2)}) %collective-permute-start) | collective-permute-done | bytes 5664 | tf_op jit(solution)/shard_map/ppermute | solution.py:56
  253.5 10.0 %convolution_convert_fusion = bf16[1024,2048]{1,0:T(8,128)(2,1)} fusion(bf16[2048,2112]{0,1:T(8,128)(2,1)} %all-gather.11.cloned.1.call-done, f32[1026,704]{0,1:T(8,128)S(1)} %maximum_convert_fusion.1, f32[1026,704]{0,1:T(8,128)S(1)} %maximum_convert_fusion, f32[704]{0:T(1024)S(1)} %get-tuple-element.120, f32[704]{0:T(1024)S(1)} %get-tuple-element.121, ...), kind=kOutput, calls=%fused_computation.13 | convolution fusion | flops 2970746880 | bytes 24412160 | tf_op jit(solution)/shard_map/dot_general | solution.py:211
  263.6 38.9 %reduce-scatter.5.cloned.1.call-done = bf16[128,2048]{1,0:T(8,128)(2,1)} async-done(((bf16[1024,2048]{1,0:T(8,128)(2,1)}), bf16[128,2048]{1,0:T(8,128)(2,1)}) %reduce-scatter.5.cloned.1.call-update) | async-done | bytes 524304 | tf_op jit(solution)/shard_map/reduce_scatter | solution.py:212
  305.2 2.2 add_convert_fusion
  (115 shorter events, 54.3 us)
Async XLA Ops:
  7.4 106.8 %copy-start = (bf16[512,2048]{1,0:T(8,128)(2,1)S(1)}, bf16[512,2048]{1,0:T(8,128)(2,1)}, u32[]{:S(2)}) copy-start(bf16[512,2048]{1,0:T(8,128)(2,1)} %param.24) | copy-start | bytes 6291460
  7.4 47.7 %all-gather.13.cloned.1.call-start = ((), (), s32[]{:S(2)}) async-start(), calls=%async_computation.7 | async-start | bytes 1310720 | tf_op jit(solution)/shard_map/all_gather | solution.py:38
  10.4 5.3 %copy-start.4 = (bf16[1024,512]{1,0:T(8,128)(2,1)S(1)}, bf16[1024,512]{1,0:T(8,128)(2,1)}, u32[]{:S(2)}) copy-start(bf16[1024,512]{1,0:T(8,128)(2,1)} %param.20) | copy-start | bytes 3145732
  14.9 0.8 copy-start.3
  17.7 10.6 %copy-start.14 = (u32[128]{0:T(128)S(1)}, u32[128]{0:T(128)}, u32[]{:S(2)}) copy-start(u32[128]{0:T(128)} %constant.99) | copy-start | bytes 1540
  17.7 41.3 %copy-start.13 = (u32[128]{0:T(128)S(1)}, u32[128]{0:T(128)}, u32[]{:S(2)}) copy-start(u32[128]{0:T(128)} %constant.104) | copy-start | bytes 1540
  28.3 55.6 %all-gather.7.cloned.1.call-start = ((), (), s32[]{:S(2)}) async-start(), calls=%async_computation.2 | async-start | bytes 1310720 | tf_op jit(solution)/shard_map/all_gather | solution.py:38
  59.0 98.4 %reduce-scatter.3.cloned.1.call-start = ((), (), s32[]{:S(2)}) async-start(), calls=%async_computation.3 | async-start | bytes 4718592 | tf_op jit(solution)/shard_map/reduce_scatter | solution.py:191
  109.7 2.2 copy-start.1
  118.5 0.9 copy-start.5
  118.5 1.0 copy-start.6
  118.5 1.1 copy-start.7
  118.5 2.1 copy-start.9
  118.5 2.1 copy-start.10
  118.5 81.2 %all-gather.11.cloned.1.call-start = ((), (), s32[]{:S(2)}) async-start(), calls=%async_computation.5 | async-start | bytes 9191424 | tf_op jit(solution)/shard_map/all_gather | solution.py:18
  119.6 43.5 %copy-start.8 = (f32[2,3,704]{2,0,1:T(2,128)S(1)}, f32[2,3,704]{2,0,1:T(2,128)}, u32[]{:S(2)}) copy-start(f32[2,3,704]{2,0,1:T(2,128)} %param.29) | copy-start | bytes 50692
  120.5 111.9 %all-gather.9.cloned.1.call-start = ((), (), s32[]{:S(2)}) async-start(), calls=%async_computation.4 | async-start | bytes 4718592 | tf_op jit(solution)/shard_map/all_gather | solution.py:200
  162.8 139.7 %reduce-scatter.5.cloned.1.call-start = ((), (), s32[]{:S(2)}) async-start(), calls=%async_computation.6 | async-start | bytes 4718592 | tf_op jit(solution)/shard_map/reduce_scatter | solution.py:212
  232.4 6.5 %copy-start.12 = (bf16[1024,2048]{1,0:T(8,128)(2,1)S(1)}, bf16[1024,2048]{1,0:T(8,128)(2,1)}, u32[]{:S(2)}) copy-start(bf16[1024,2048]{1,0:T(8,128)(2,1)} %all-gather.9.cloned.1.call-done) | copy-start | bytes 12582916
  239.0 8.9 %copy-start.11 = (f32[2,704]{1,0:T(2,128)S(1)}, f32[2,704]{1,0:T(2,128)}, u32[]{:S(2)}) copy-start(f32[2,704]{1,0:T(2,128)} %param.30) | copy-start | bytes 16900
  244.3 7.6 %collective-permute-start = (bf16[4,704]{0,1:T(8,128)(2,1)S(1)}, bf16[4,704]{0,1:T(8,128)(2,1)S(1)}, u32[]{:S(2)}, u32[]{:S(2)}) collective-permute-start(bf16[4,704]{0,1:T(8,128)(2,1)S(1)} %pad_maximum_fusion.1), channel_id=1, source_target_pairs={{0,8},{8,16},{16,24},{24,32},{32,40},{40,48},{48,56},{56,64},{64,7... | collective-permute-start | bytes 16904 | tf_op jit(solution)/shard_map/ppermute | solution.py:56
  263.5 39.0 %copy-start.2 = (bf16[128,2048]{1,0:T(8,128)(2,1)S(1)}, bf16[128,2048]{1,0:T(8,128)(2,1)}, u32[]{:S(2)}) copy-start(bf16[128,2048]{1,0:T(8,128)(2,1)} %add_convert_fusion.1) | copy-start | bytes 1572868
Sparse Core Ops, SparseCore 0:
  28.4 26.5 all-gather.12
  59.1 24.6 all-gather.6
  118.7 38.6 reduce-scatter.2
  263.7 38.7 reduce-scatter.4
Sparse Core Ops, SparseCore 1:
  121.1 78.5 all-gather.10
  201.3 31.1 all-gather.8
where the time goes:
time: 316 us; the launch traced here: 314 us
  waiting for transfers between devices  165 us (52%)
  other arithmetic  51.6 us (16%)
  matrix products  39.7 us (13%)
  blocking collectives  21.5 us (7%)
  between operations  20.6 us (7%)
  local copies, waits for them, and re-layouts  12.4 us (4%)
  starting transfers between devices  4.01 us (1%)
    reduce_scatter x1, waiting for transfers between devices, shards(): lax.psum_scatter(partial_ffn.astype(jnp.bfloat16), 'tp', scatter_dimensio...  38.9 us
    reduce_scatter x1, waiting for transfers between devices, shards(): lax.psum_scatter(partial_rows.astype(jnp.bfloat16), 'tp', scatter_dimensi...  36.8 us
    all_gather x1, waiting for transfers between devices, turned_gather(): out, at, finished = (lax.all_gather(both, axis, axis=0, tiled=True), 0, [])  36.6 us
    all_gather x1, waiting for transfers between devices, shards(): whole_rows = lax.all_gather(normed_own, 'tp', axis=0, tiled=True)  32.7 us
    unnamed x2, blocking collectives  21.5 us
    all_gather x2, waiting for transfers between devices, entering(): lax.all_gather(part.astype(kind), axis)  15.5 us
    dot_general x1, matrix products, shards(): jnp.dot(activated, full_down, preferred_element_type=jnp.float32)  10 us
    dot_general x4, matrix products, advance(): jnp.einsum('thd,hde->the', pieces[0], carry_state.astype(jnp.bfloat16), p...  7.74 us
  transfers between devices with their start and end apart: 7, of which 7 were waited for; matrix products, arithmetic and copies ran while one was open for 5% of the time, Pallas kernels for 0%

commit v1 on v0

--- a/solution.py
+++ b/solution.py
@@ -15,7 +15,13 @@
 def turned_gather(arrays, axis, dims):
     turned = [jnp.moveaxis(a, dim, 0) for a, dim in zip(arrays, dims)]
     both = jnp.concatenate([t.reshape(len(t), -1) for t in turned], axis=1)
-    out, at, finished = (lax.all_gather(both, axis, axis=0, tiled=True), 0, [])
+    out, at, finished = (
+        jnp.concatenate(
+            lax.all_to_all(jnp.stack([both] * lax.axis_size(axis)), axis, 0, 0), axis=0
+        ),
+        0,
+        [],
+    )
     for t, dim in zip(turned, dims):
         piece = out[:, at : at + t[0].size].reshape(-1, *t.shape[1:])
         finished.append(jnp.moveaxis(piece, 0, dim))

time: 316 us -> 358 us (1.13)
  local copies, waits for them, and re-layouts: 12.4 us -> 29.1 us
  waiting for transfers between devices: 165 us -> 179 us
  matrix products: 39.7 us -> 45.4 us
  starting transfers between devices: 4.01 us -> 7.95 us
    all_to_all x0 -> x1, waiting for transfers between devices: none -> 92.9 us  [turned_gather(): lax.all_to_all(jnp.stack([both] * lax.axis_size(axis)), axis, 0, 0)]
    all_gather x1 -> x0, waiting for transfers between devices: 36.6 us -> none  [turned_gather(): out, at, finished = (lax.all_gather(both, axis, axis=0, tiled=True), 0, [])]
    all_gather x1, waiting for transfers between devices: 32.7 us -> 0.01 us  [shards(): whole_rows = lax.all_gather(normed_own, 'tp', axis=0, tiled=True)]
    all_to_all x0 -> x1, local copies, waits for them, and re-layouts: none -> 11.7 us  [turned_gather(): lax.all_to_all(jnp.stack([both] * lax.axis_size(axis)), axis, 0, 0)]
    reduce_scatter x1, waiting for transfers between devices: 36.8 us -> 26.5 us  [shards(): lax.psum_scatter(partial_rows.astype(jnp.bfloat16), 'tp', scatter_dimensi...]
    dot_general x1, matrix products: 10 us -> 16.3 us  [shards(): jnp.dot(activated, full_down, preferred_element_type=jnp.float32)]
    all_to_all x0 -> x1, starting transfers between devices: none -> 6.08 us  [turned_gather(): lax.all_to_all(jnp.stack([both] * lax.axis_size(axis)), axis, 0, 0)]
    another operation x4 -> x5, local copies, waits for them, and re-layouts: 0.23 us -> 5.19 us  [the longest x1 4.96 us: turned_gather(): jnp.stack([both] * lax.axis_size(axis))]
  transfers between devices with their start and end apart: 7 -> 7, of which waited for: 7 -> 6; matrix products, arithmetic and copies ran while one was open for 5% -> 9% of each run, Pallas kernels for 0% -> 0%
where the time goes in v1:
time: 358 us; the launch traced here: 356 us
  waiting for transfers between devices  179 us (50%)
  other arithmetic  54.1 us (15%)
  matrix products  45.4 us (13%)
  local copies, waits for them, and re-layouts  29.1 us (8%)
  blocking collectives  21.5 us (6%)
  between operations  19.1 us (5%)
  starting transfers between devices  7.95 us (2%)
    all_to_all x1, waiting for transfers between devices, turned_gather(): lax.all_to_all(jnp.stack([both] * lax.axis_size(axis)), axis, 0, 0)  92.9 us
    reduce_scatter x1, waiting for transfers between devices, shards(): lax.psum_scatter(partial_ffn.astype(jnp.bfloat16), 'tp', scatter_dimensio...  41 us
    reduce_scatter x1, waiting for transfers between devices, shards(): lax.psum_scatter(partial_rows.astype(jnp.bfloat16), 'tp', scatter_dimensi...  26.5 us
    unnamed x2, blocking collectives  21.5 us
    dot_general x1, matrix products, shards(): jnp.dot(activated, full_down, preferred_element_type=jnp.float32)  16.3 us
    all_gather x2, waiting for transfers between devices, entering(): lax.all_gather(part.astype(kind), axis)  15.5 us
    all_to_all x1, local copies, waits for them, and re-layouts, turned_gather(): lax.all_to_all(jnp.stack([both] * lax.axis_size(axis)), axis, 0, 0)  11.7 us
    dot_general x4, matrix products, advance(): jnp.einsum('thd,hde->the', pieces[0], carry_state.astype(jnp.bfloat16), p...  7.76 us
  transfers between devices with their start and end apart: 7, of which 6 were waited for; matrix products, arithmetic and copies ran while one was open for 9% of the time, Pallas kernels for 0%

profile of v1, /device:TPU:0, one launch (start us, length us, event | category | flops | bytes accessed | tf_op | source)
XLA Modules:
  0.0 356.1 jit_solution(813721763161240955)
XLA Ops:
  6.5 2.4 reduce-window.6
  11.0 3.1 fusion.56
  16.9 9.8 %while.24 = (s32[]{:T(128)}, f32[1,256,512]{2,1,0:T(8,128)S(1)}, f32[4,1]{0,1:T(1,128)S(1)}, f32[4,1,256,512]{3,2,1,0:T(8,128)}, s32[]{:T(128)}, /*index=5*/s32[]{:T(128)}) while((s32[]{:T(128)}, f32[1,256,512]{2,1,0:T(8,128)S(1)}, f32[4,1]{0,1:T(1,128)S(1)}, f32[4,1,256,512]{3,2,1,0:T(8,128)}, s32[]{:T(128)}, ...), condition=%wide.region_4.5_spmd.clone, body=%wide.region_3.4_spmd.clone.sunk | while | flops 393219 | bytes 1572971 | solution.py:169
  30.2 10.8 %all-reduce = bf16[4]{0:T(256)(128)(2,1)S(1)} all-reduce(bf16[4]{0:T(256)(128)(2,1)S(1)} %dynamic-update-slice), channel_id=1, replica_groups=mesh['sp_0'=4,'sp_1'=4,'tp'=8] {'sp_1'}, use_global_device_ids=true, to_apply=%add | all-reduce | flops 4 | bytes 16
  42.3 11.9 %all-gather.10.cloned.1.call-done = bf16[4,256,512]{2,1,0:T(8,128)(2,1)} async-done(((bf16[1,256,512]{2,1,0:T(8,128)(2,1)}), bf16[4,256,512]{2,1,0:T(8,128)(2,1)}) %all-gather.10.cloned.1.call-update) | async-done | bytes 1048592 | tf_op jit(solution)/shard_map/all_gather | solution.py:44
  54.2 4.0 %fusion.70 = bf16[1,1,256,512]{3,2,1,0:T(8,128)(2,1)} fusion(f32[]{:T(128)} %bitcast.39, f32[]{:T(128)} %bitcast.40, f32[]{:T(128)} %bitcast.41, f32[]{:T(128)} %bitcast.42, bf16[4,256,512]{2,1,0:T(8,128)(2,1)} %all-gather.10.cloned.1.call-done), kind=kLoop, calls=%fused_computation.102 | loop fusion | flops 1572864 | bytes 1310736 | tf_op jit(solution)/shard_map/convert_element_type | solution.py:44
  61.0 10.7 %all-reduce.1 = bf16[4]{0:T(256)(128)(2,1)S(1)} all-reduce(bf16[4]{0:T(256)(128)(2,1)S(1)} %dynamic-update-slice.1), channel_id=2, replica_groups=mesh['sp_0'=4,'sp_1'=4,'tp'=8] {'sp_0'}, use_global_device_ids=true, to_apply=%add.1 | all-reduce | flops 4 | bytes 16
  79.3 3.6 %all-gather.6.cloned.1.call-done = bf16[4,1,256,512]{3,2,1,0:T(8,128)(2,1)} async-done(((bf16[1,1,256,512]{3,2,1,0:T(8,128)(2,1)}), bf16[4,1,256,512]{3,2,1,0:T(8,128)(2,1)}) %all-gather.6.cloned.1.call-update) | async-done | bytes 1048592 | tf_op jit(solution)/shard_map/all_gather | solution.py:44
  83.0 3.9 %fusion.69 = f32[1,256,512]{2,1,0:T(8,128)S(1)} fusion(bf16[4,1,256,512]{3,2,1,0:T(8,128)(2,1)} %all-gather.6.cloned.1.call-done, f32[]{:T(128)} %bitcast.39, f32[]{:T(128)} %bitcast.40, f32[]{:T(128)} %bitcast.41, f32[]{:T(128)} %bitcast.42, f32[]{:T(128)} %bitcast.33, f32[]{:T(128)S(6)} %convert.26, f32[]{:T(128)S(6)} %convert.27, f32[]{:T(128)} %bitcast.38, ...), kind=kLoop, calls=%fused_computation.99 | loop fusion | flops 4194304 | bytes 2621484 | tf_op jit(solution)/shard_map/add | solution.py:122
  86.9 17.8 %while.23 = (s32[]{:T(128)}, f32[1,256,512]{2,1,0:T(8,128)S(1)}, f32[4,256,1,512]{3,1,2,0:T(8,128)}, f32[4,1]{0,1:T(1,128)S(1)}, f32[4,1,256,512]{3,2,1,0:T(8,128)}, /*index=5*/bf16[4,256,1,256]{3,1,2,0:T(8,128)(2,1)}, s32[]{:T(128)}) while((s32[]{:T(128)}, f32[1,256,512]{2,1,0:T(8,128)S(1)}, f32[4,256,1,512]{3,1,2,0:T(8,128)}, ...), condition=%wide.region_6.7_spmd, body=%wide.region_5.6_spmd.sunk | while | flops 67502080 | bytes 2753641 | solution.py:184
  104.7 4.2 %fusion.102 = (f32[4,256]{1,0:T(4,128)S(1)}, f32[4,256,1,512]{3,1,0,2:T(8,128)}) fusion(f32[4,256,1,512]{3,1,2,0:T(8,128)} %get-tuple-element.60, bf16[4,256,512]{2,1,0:T(8,128)(2,1)} %bitcast.154, bf16[4,256,128]{2,1,0:T(8,128)(2,1)} %bitcast.159, bf16[4,256,128]{2,1,0:T(8,128)(2,1)S(1)} %bitcast.157, f32[4,256]{1,0:T(4,128)S(1)} %get-tuple-element.155, ...), kind=kOutput, calls=%fused_computation.160 | convolution fusion | flops 406846464 | bytes 6889472 | tf_op jit(solution)/shard_map/vmap(htm,mhe->the)/dot_general | solution.py:96
  113.3 4.3 %convolution_convert_fusion.1 = bf16[1024,2048]{1,0:T(8,128)(2,1)} fusion(bf16[1024,512]{1,0:T(8,128)(2,1)S(1)} %fusion.31, bf16[512,2048]{1,0:T(8,128)(2,1)S(1)} %copy-done), kind=kOutput, calls=%fused_computation.14 | convolution fusion | flops 2149580800 | bytes 7340032 | tf_op jit(solution)/shard_map/dot_general | solution.py:196
  118.8 5.0 %stack.2 = bf16[16,128,2112]{1,2,0:T(8,128)(2,1)} broadcast(bf16[128,2112]{0,1:T(8,128)(2,1)S(1)} %pad_maximum_fusion), dimensions={1,2} | broadcast | bytes 9191424 | tf_op jit(solution)/shard_map/stack | solution.py:20
  123.7 6.1 %all-to-all-start = ((bf16[16,128,2112]{1,2,0:T(8,128)(2,1)}), bf16[16,128,2112]{1,2,0:T(8,128)(2,1)}, u32[]{:S(2)}, u32[]{:S(2)}) async-start(bf16[16,128,2112]{1,2,0:T(8,128)(2,1)} %stack.2), calls=%async_computation.1 | async-start | bytes 17301504 | tf_op jit(solution)/shard_map/all_to_all | solution.py:20
  130.0 26.5 %reduce-scatter.3.cloned.1.call-done = bf16[128,2048]{1,0:T(8,128)(2,1)} async-done(((bf16[1024,2048]{1,0:T(8,128)(2,1)}), bf16[128,2048]{1,0:T(8,128)(2,1)}) %reduce-scatter.3.cloned.1.call-update) | async-done | bytes 524304 | tf_op jit(solution)/shard_map/reduce_scatter | solution.py:197
  162.1 92.9 %all-to-all-done = bf16[16,128,2112]{1,2,0:T(8,128)(2,1)} async-done(((bf16[16,128,2112]{1,2,0:T(8,128)(2,1)}), bf16[16,128,2112]{1,2,0:T(8,128)(2,1)}, u32[]{:S(2)}, u32[]{:S(2)}) %all-to-all-start) | async-done | bytes 8650784 | tf_op jit(solution)/shard_map/all_to_all | solution.py:20
  255.1 11.7 %copy.70 = bf16[16,128,2112]{2,1,0:T(8,128)(2,1)} copy(bf16[16,128,2112]{1,2,0:T(8,128)(2,1)} %all-to-all-done) | data formatting | bytes 17301504 | tf_op jit(solution)/shard_map/all_to_all | solution.py:20
  266.8 7.4 %fusion.35 = bf16[1024,704]{0,1:T(8,128)(2,1)S(1)} fusion(bf16[1024,2048]{1,0:T(8,128)(2,1)} %all-gather.8.cloned.1.call-done, bf16[2048,2112]{1,0:T(8,128)(2,1)} %bitcast.147), kind=kOutput, calls=%fused_computation.53 | convolution fusion | flops 2953510912 | bytes 8781824 | tf_op jit(solution)/shard_map/dot_general | solution.py:208
  274.4 3.3 fusion.32
  279.5 2.7 collective-permute-done
  282.4 2.5 maximum_convert_fusion.1
  284.9 2.5 maximum_convert_fusion
  287.4 16.3 %convolution_convert_fusion = bf16[1024,2048]{1,0:T(8,128)(2,1)} fusion(bf16[2048,2112]{1,0:T(8,128)(2,1)S(1)} %bitcast.149, f32[1026,704]{0,1:T(8,128)} %maximum_convert_fusion.1, f32[1026,704]{0,1:T(8,128)} %maximum_convert_fusion, f32[704]{0:T(1024)S(1)} %get-tuple-element.130, f32[704]{0:T(1024)S(1)} %get-tuple-element.131, ...), kind=kOutput, calls=%fused_computation.13 | convolution fusion | flops 2970746880 | bytes 24674304 | tf_op jit(solution)/shard_map/dot_general | solution.py:217
  303.7 41.0 %reduce-scatter.5.cloned.1.call-done = bf16[128,2048]{1,0:T(8,128)(2,1)} async-done(((bf16[1024,2048]{1,0:T(8,128)(2,1)}), bf16[128,2048]{1,0:T(8,128)(2,1)}) %reduce-scatter.5.cloned.1.call-update) | async-done | bytes 524304 | tf_op jit(solution)/shard_map/reduce_scatter | solution.py:218
  (120 shorter events, 60.0 us)
Async XLA Ops:
  6.5 106.8 %copy-start = (bf16[512,2048]{1,0:T(8,128)(2,1)S(1)}, bf16[512,2048]{1,0:T(8,128)(2,1)}, u32[]{:S(2)}) copy-start(bf16[512,2048]{1,0:T(8,128)(2,1)} %param.24) | copy-start | bytes 6291460
  6.5 47.6 %all-gather.10.cloned.1.call-start = ((), (), s32[]{:S(2)}) async-start(), calls=%async_computation.7 | async-start | bytes 1310720 | tf_op jit(solution)/shard_map/all_gather | solution.py:44
  9.5 5.3 %copy-start.6 = (bf16[1024,512]{1,0:T(8,128)(2,1)S(1)}, bf16[1024,512]{1,0:T(8,128)(2,1)}, u32[]{:S(2)}) copy-start(bf16[1024,512]{1,0:T(8,128)(2,1)} %param.20) | copy-start | bytes 3145732
  14.0 0.8 copy-start.5
  16.9 10.6 %copy-start.16 = (u32[128]{0:T(128)S(1)}, u32[128]{0:T(128)}, u32[]{:S(2)}) copy-start(u32[128]{0:T(128)} %constant.99) | copy-start | bytes 1540
  16.9 41.3 %copy-start.15 = (u32[128]{0:T(128)S(1)}, u32[128]{0:T(128)}, u32[]{:S(2)}) copy-start(u32[128]{0:T(128)} %constant.104) | copy-start | bytes 1540
  27.4 55.6 %all-gather.6.cloned.1.call-start = ((), (), s32[]{:S(2)}) async-start(), calls=%async_computation.3 | async-start | bytes 1310720 | tf_op jit(solution)/shard_map/all_gather | solution.py:44
  58.2 98.3 %reduce-scatter.3.cloned.1.call-start = ((), (), s32[]{:S(2)}) async-start(), calls=%async_computation.4 | async-start | bytes 4718592 | tf_op jit(solution)/shard_map/reduce_scatter | solution.py:197
  108.9 2.2 copy-start.2
  117.6 0.9 copy-start.7
  117.6 1.0 copy-start.8
  117.6 1.1 copy-start.9
  123.7 6.2 %copy-start.11 = (f32[2,2048]{1,0:T(2,128)S(1)}, f32[2,2048]{1,0:T(2,128)}, u32[]{:S(2)}) copy-start(f32[2,2048]{1,0:T(2,128)} %param.26) | copy-start | bytes 49156
  123.7 6.2 %copy-start.12 = (f32[2,2048]{1,0:T(2,128)S(1)}, f32[2,2048]{1,0:T(2,128)}, u32[]{:S(2)}) copy-start(f32[2,2048]{1,0:T(2,128)} %param.25) | copy-start | bytes 49156
  123.7 131.3 %all-to-all-start = ((bf16[16,128,2112]{1,2,0:T(8,128)(2,1)}), bf16[16,128,2112]{1,2,0:T(8,128)(2,1)}, u32[]{:S(2)}, u32[]{:S(2)}) async-start(bf16[16,128,2112]{1,2,0:T(8,128)(2,1)} %stack.2), calls=%async_computation.1 | async-start | bytes 17301504 | tf_op jit(solution)/shard_map/all_to_all | solution.py:20
  129.8 32.2 %copy-start.10 = (f32[2,3,704]{2,0,1:T(2,128)S(1)}, f32[2,3,704]{2,0,1:T(2,128)}, u32[]{:S(2)}) copy-start(f32[2,3,704]{2,0,1:T(2,128)} %param.29) | copy-start | bytes 50692
  129.8 136.9 %all-gather.8.cloned.1.call-start = ((), (), s32[]{:S(2)}) async-start(), calls=%async_computation.5 | async-start | bytes 4718592 | tf_op jit(solution)/shard_map/all_gather | solution.py:206
  161.8 182.9 %reduce-scatter.5.cloned.1.call-start = ((), (), s32[]{:S(2)}) async-start(), calls=%async_computation.6 | async-start | bytes 4718592 | tf_op jit(solution)/shard_map/reduce_scatter | solution.py:218
  266.8 7.6 %copy-start.4 = (bf16[16,128,2112]{2,1,0:T(8,128)(2,1)S(1)}, bf16[16,128,2112]{2,1,0:T(8,128)(2,1)}, u32[]{:S(2)}) copy-start(bf16[16,128,2112]{2,1,0:T(8,128)(2,1)} %copy.70) | copy-start | bytes 25952260
  266.8 7.6 %copy-start.14 = (bf16[1024,2048]{1,0:T(8,128)(2,1)S(1)}, bf16[1024,2048]{1,0:T(8,128)(2,1)}, u32[]{:S(2)}) copy-start(bf16[1024,2048]{1,0:T(8,128)(2,1)} %all-gather.8.cloned.1.call-done) | copy-start | bytes 12582916
  274.4 5.2 %copy-start.13 = (f32[2,704]{1,0:T(2,128)S(1)}, f32[2,704]{1,0:T(2,128)}, u32[]{:S(2)}) copy-start(f32[2,704]{1,0:T(2,128)} %param.30) | copy-start | bytes 16900
  278.0 4.3 %collective-permute-start = (bf16[4,704]{0,1:T(8,128)(2,1)S(1)}, bf16[4,704]{0,1:T(8,128)(2,1)S(1)}, u32[]{:S(2)}, u32[]{:S(2)}) collective-permute-start(bf16[4,704]{0,1:T(8,128)(2,1)S(1)} %pad_maximum_fusion.1), channel_id=1, source_target_pairs={{0,8},{8,16},{16,24},{24,32},{32,40},{40,48},{48,56},{56,64},{64,7... | collective-permute-start | bytes 16904 | tf_op jit(solution)/shard_map/ppermute | solution.py:62
  303.7 41.1 %copy-start.3 = (bf16[128,2048]{1,0:T(8,128)(2,1)S(1)}, bf16[128,2048]{1,0:T(8,128)(2,1)}, u32[]{:S(2)}) copy-start(bf16[128,2048]{1,0:T(8,128)(2,1)} %add_convert_fusion.1) | copy-start | bytes 1572868
  303.7 45.9 %copy-start.1 = (bf16[512,2048]{1,0:T(8,128)(2,1)S(1)}, bf16[512,2048]{1,0:T(8,128)(2,1)}, u32[]{:S(2)}) copy-start(bf16[512,2048]{1,0:T(8,128)(2,1)} %param.24) | copy-start | bytes 6291460
Sparse Core Ops, SparseCore 0:
  27.5 26.5 all-gather.9
  58.3 24.6 all-gather.5
  117.8 38.6 reduce-scatter.2
  162.0 31.2 all-gather.7
  303.8 40.8 reduce-scatter.4
